TPU v7x, 32 devices: a whole 2x2x4 slice. The times are simulated.
32 devices in a mesh: sp: 8 (over z, y), tp: 4 (over x, core).
Axes of the slice: x: 2, y: 2, z: 4, core: 2. Of those that a mesh axis runs over, the one named last changes fastest.
Arguments:
- skip_stream_vector: bfloat16 [8192, 2048], P(('sp', 'tp')), may hold values from -6 to 6
- probe_preactivation: bfloat16 [8192, 1024], P('sp', 'tp'), may hold values from -6 to 6
- retention_preactivation: bfloat16 [8192, 1024], P('sp', 'tp'), may hold values from -4.5 to 4.5
- content_vector: bfloat16 [8192, 1024], P('sp', 'tp'), may hold values from -6 to 6
- emission_preactivation: bfloat16 [8192, 1024], P('sp', 'tp'), may hold values from -6 to 6
- retention_slack: float32 [1024], P('tp'), may hold values from 0 to 0.12
- surge_rate: float32 [8192, 1024], P('sp', 'tp'), may hold values from -1.2 to 0
- subspace_scaling_factor: float32 [1024], P('tp'), may hold values from 0.1 to 1.9
- emission_matrix: bfloat16 [1024, 2048], replicated, may hold values from -0.1875 to 0.1875
- mlp_scaling_factor: float32 [2048], replicated, may hold values from 0.1 to 1.9
- switch_matrix: bfloat16 [2048, 5632], P('sp', 'tp'), may hold values from -0.125 to 0.125
- expansion_matrix: bfloat16 [2048, 5632], P('sp', 'tp'), may hold values from -0.125 to 0.125
- contraction_matrix: bfloat16 [5632, 2048], P('tp', 'sp'), may hold values from -0.078125 to 0.078125
Outputs:
- stream_out: bfloat16 [8192, 2048], P(('sp', 'tp'))
All inputs are finite; a program needn't handle non-finite values.
Results may differ from a plain program's by a relative error of at most 0.017.
Values may be sent and summed in bfloat16 or wider, within the bound.
A program may use at most 128 MiB of HBM per device.

v0:
```python
import jax
import jax.numpy as jnp
from jax import lax
from jax.sharding import PartitionSpec as P

HEAD_DIM = 128
BLOCK = 64


EPSILON = 1e-06
TOP_PRECISION = lax.Precision.HIGHEST


def carried_in(value, axis, join, neutral):
    place = lax.axis_index(axis)
    gathered = jax.tree.map(
        lambda a, kind: lax.all_gather(a.astype(kind), axis), value, (jnp.bfloat16, jnp.bfloat16)
    )
    state = jax.tree.map(lambda a, e: jnp.zeros_like(a) + jnp.asarray(e, a.dtype), value, neutral)

    def one(turn, state):
        return join(
            state,
            jax.tree.map(
                lambda a, own: lax.dynamic_index_in_dim(a, turn, 0, False).astype(own.dtype),
                gathered,
                value,
            ),
        )

    return lax.fori_loop(0, place, one, state)


def block_step(carry, inputs):
    memory_state, offsets = carry
    query_block, input_gate_block, value_block, log_blk = inputs
    cumulative_decay = jnp.cumsum(log_blk, axis=1)
    length = log_blk.shape[1]
    carried_share = jnp.einsum(
        "eia,eax->eix",
        query_block * jnp.exp(cumulative_decay),
        memory_state,
        precision=TOP_PRECISION,
    )
    middle = cumulative_decay[:, length // 2, :][:, None, :]
    left_side = query_block * jnp.exp(cumulative_decay - middle)
    right_side = input_gate_block * jnp.exp(middle - cumulative_decay)
    causal = (jnp.arange(length)[:, None] >= jnp.arange(length)[None, :])[None, :, :]
    scores = jnp.einsum("htk,hsk->hts", left_side, right_side, precision=TOP_PRECISION)
    scores = jnp.where(causal, scores, 0.0)
    outputs = carried_share + jnp.einsum(
        "hts,hsv->htv", scores, value_block, precision=TOP_PRECISION
    )
    closing_log_decay = cumulative_decay[:, -1, :]
    updated_memory_state = jnp.exp(closing_log_decay)[:, :, None] * memory_state + jnp.einsum(
        "qnj,qnl->qjl",
        input_gate_block * jnp.exp(closing_log_decay[:, None, :] - cumulative_decay),
        value_block,
        precision=TOP_PRECISION,
    )
    return (
        (updated_memory_state, offsets + closing_log_decay),
        (outputs, cumulative_decay + offsets[:, None, :]),
    )


def split_blocks(values, heads_here):
    count = values.shape[0]
    return values.reshape(count // BLOCK, BLOCK, heads_here, HEAD_DIM).transpose(0, 2, 1, 3)


def admission_source_matrix(
    probe_preactivation, retention_preactivation, content_vector, retention_slack, surge_rate
):
    query_act = jax.nn.silu(probe_preactivation.astype(jnp.float32))
    admission_factor = retention_slack[None, :] * jax.nn.sigmoid(
        -retention_preactivation.astype(jnp.float32)
    )
    retention_logarithm = jnp.log1p(-admission_factor) + surge_rate
    return (query_act, admission_factor, content_vector.astype(jnp.float32), retention_logarithm)


def head_output(outputs, subspace_scaling_factor, emission_preactivation):
    count, heads_here = (outputs.shape[0], outputs.shape[1])
    squares = jnp.mean(outputs * outputs, axis=-1, keepdims=True)
    scaled = (
        outputs
        * lax.rsqrt(squares + EPSILON)
        * subspace_scaling_factor.reshape(heads_here, HEAD_DIM)
    )
    scaled = scaled.reshape(count, heads_here * HEAD_DIM)
    return (scaled * jax.nn.silu(emission_preactivation.astype(jnp.float32))).astype(jnp.bfloat16)


def row_norm(stream, mlp_scaling_factor):
    streamf = stream.astype(jnp.float32)
    squares = jnp.mean(streamf * streamf, axis=-1, keepdims=True)
    return (streamf * lax.rsqrt(squares + EPSILON) * mlp_scaling_factor).astype(jnp.bfloat16)


def chain(earlier, later):
    return (earlier[0] * later[0], later[0][:, :, None] * earlier[1] + later[1])


def on_device(
    skip_stream_vector,
    probe_preactivation,
    retention_preactivation,
    content_vector,
    emission_preactivation,
    retention_slack,
    surge_rate,
    subspace_scaling_factor,
    emission_matrix,
    mlp_scaling_factor,
    switch_matrix,
    expansion_matrix,
    contraction_matrix,
):
    heads_here = probe_preactivation.shape[1] // HEAD_DIM
    tok_rows = probe_preactivation.shape[0]
    arranged_sources = admission_source_matrix(
        probe_preactivation, retention_preactivation, content_vector, retention_slack, surge_rate
    )
    block_list = tuple((split_blocks(item, heads_here) for item in arranged_sources))
    start_carry = (
        jnp.zeros((heads_here, HEAD_DIM, HEAD_DIM), jnp.float32),
        jnp.zeros((heads_here, HEAD_DIM), jnp.float32),
    )
    (memory_state, offsets), (outputs, cumulative_log_decay) = lax.scan(
        block_step, start_carry, block_list
    )
    incoming_state = carried_in(
        (jnp.exp(offsets), memory_state),
        "sp",
        chain,
        (jnp.ones_like(offsets), jnp.zeros_like(memory_state)),
    )
    outputs = outputs + jnp.einsum(
        "jmxo,mos->jmxs",
        block_list[0] * jnp.exp(cumulative_log_decay),
        incoming_state[1],
        precision=TOP_PRECISION,
    )
    outputs = outputs.transpose(0, 2, 1, 3).reshape(tok_rows, heads_here, HEAD_DIM)
    mixed = head_output(outputs, subspace_scaling_factor, emission_preactivation)
    own_width = heads_here * HEAD_DIM
    own_rows = lax.dynamic_slice_in_dim(
        emission_matrix, lax.axis_index("tp") * own_width, own_width, 0
    )
    projected = lax.psum_scatter(
        jnp.dot(mixed, own_rows, preferred_element_type=jnp.float32).astype(jnp.bfloat16),
        "tp",
        scatter_dimension=0,
        tiled=True,
    ).astype(jnp.float32)
    stream = (skip_stream_vector.astype(jnp.float32) + projected).astype(jnp.bfloat16)
    normed = row_norm(stream, mlp_scaling_factor)
    all_rows = lax.all_gather(normed, "tp", axis=0, tiled=True)
    gate_proj = jnp.dot(
        all_rows,
        lax.all_gather(switch_matrix, "sp", axis=0, tiled=True),
        preferred_element_type=jnp.float32,
    )
    up_proj = jnp.dot(
        all_rows,
        lax.all_gather(expansion_matrix, "sp", axis=0, tiled=True),
        preferred_element_type=jnp.float32,
    )
    hidden = (jax.nn.silu(gate_proj) * up_proj).astype(jnp.bfloat16)
    partial_sum = jnp.dot(
        hidden,
        lax.all_gather(contraction_matrix, "sp", axis=1, tiled=True),
        preferred_element_type=jnp.float32,
    )
    summed = lax.psum_scatter(
        partial_sum.astype(jnp.bfloat16), "tp", scatter_dimension=0, tiled=True
    ).astype(jnp.float32)
    return (stream.astype(jnp.float32) + summed).astype(jnp.bfloat16)


def solution(mesh):
    in_specs = (
        P(("sp", "tp"), None),
        P("sp", "tp"),
        P("sp", "tp"),
        P("sp", "tp"),
        P("sp", "tp"),
        P("tp"),
        P("sp", "tp"),
        P("tp"),
        P(),
        P(),
        P("sp", "tp"),
        P("sp", "tp"),
        P("tp", "sp"),
    )
    out_specs = P(("sp", "tp"), None)
    return jax.shard_map(
        on_device, mesh=mesh, in_specs=in_specs, out_specs=out_specs, check_vma=False
    )
```

profile of v0, /device:TPU:27, one launch (start us, length us, event | category | flops | bytes accessed | tf_op | source)
XLA Modules:
  0.0 519.6 jit_solution(11291250167391390919)
XLA Ops:
  7.4 2.0 divide_multiply_fusion
  9.9 1.5 reshape.84
  11.4 1.3 convert_multiply_fusion.3
  13.4 2.5 reshape.90
  16.0 55.3 %while.30 = (s32[]{:T(128)}, f32[2,128,128]{2,1,0:T(8,128)S(1)}, f32[2,128]{1,0:T(2,128)S(1)}, f32[16,2,64,128]{3,2,0,1:T(8,128)}, f32[16,2,64,128]{3,2,1,0:T(8,...) while((s32[]{:T(128)}, f32[2,128,128]{2,1,0:T(8,128)S(1)}, ...), condition=%wide.region_2.3_spmd.clone, body=%wide.region_0.2_spmd.clone.sunk | while | flops 76820992 | bytes 2124949 | solution.py:130
  16.1 0.9 constant_dynamic-slice_fusion.6
  19.6 0.9 constant_dynamic-slice_fusion.6
  23.0 0.9 constant_dynamic-slice_fusion.6
  26.5 0.9 constant_dynamic-slice_fusion.6
  29.9 0.9 constant_dynamic-slice_fusion.6
  33.4 0.9 constant_dynamic-slice_fusion.6
  36.8 0.9 constant_dynamic-slice_fusion.6
  40.3 0.9 constant_dynamic-slice_fusion.6
  43.8 0.9 constant_dynamic-slice_fusion.6
  47.2 0.9 constant_dynamic-slice_fusion.6
  71.3 23.1 %all-gather.1 = bf16[16,128,128]{2,1,0:T(8,128)(2,1)S(1)} all-gather(bf16[2,128,128]{2,1,0:T(8,128)(2,1)S(1)} %convert_element_type.72), channel_id=3, replica_groups=mesh['sp'=8,'tp'=4] {'sp'}, dimensions={0}, use_global_device_ids=true | all-gather | bytes 589824 | tf_op jit(solution)/shard_map/all_gather | solution.py:17
  94.4 14.8 %all-gather.2 = bf16[8,2,128]{2,1,0:T(2,128)(2,1)S(1)} all-gather(bf16[1,2,128]{2,1,0:T(2,128)(2,1)S(1)} %fusion.44), channel_id=2, replica_groups=mesh['sp'=8,'tp'=4] {'sp'}, dimensions={0}, use_global_device_ids=true | all-gather | bytes 4608 | tf_op jit(solution)/shard_map/all_gather | solution.py:17
  109.1 1.0 while.29
  110.2 2.8 multiply_reduce_fusion
  114.1 1.2 mul.112
  115.4 4.6 convolution_convert_fusion.1
  120.7 53.7 %reduce-scatter.3.cloned.1.call-done = bf16[256,2048]{1,0:T(8,128)(2,1)} async-done(((bf16[1024,2048]{1,0:T(8,128)(2,1)}), bf16[256,2048]{1,0:T(8,128)(2,1)}) %reduce-scatter.3.cloned.1.call-update) | async-done | bytes 1048592 | tf_op jit(solution)/shard_map/reduce_scatter | solution.py:151
  174.4 1.8 fusion.23
  176.2 2.6 fusion.25
  180.3 43.4 %all-gather.10.cloned.1.call-done = bf16[2048,1408]{1,0:T(8,128)(2,1)} async-done(((bf16[256,1408]{1,0:T(8,128)(2,1)}), bf16[2048,1408]{1,0:T(8,128)(2,1)}) %all-gather.10.cloned.1.call-update) | async-done | bytes 5767184 | tf_op jit(solution)/shard_map/all_gather | solution.py:162
  223.7 35.2 %all-gather.8.cloned.1.call-done = bf16[1024,2048]{1,0:T(8,128)(2,1)} async-done(((bf16[256,2048]{1,0:T(8,128)(2,1)}), bf16[1024,2048]{1,0:T(8,128)(2,1)}) %all-gather.8.cloned.1.call-update) | async-done | bytes 4194320 | tf_op jit(solution)/shard_map/all_gather | solution.py:159
  259.0 11.7 %fusion.49 = f32[1024,1408]{1,0:T(8,128)} fusion(bf16[1024,2048]{1,0:T(8,128)(2,1)} %all-gather.8.cloned.1.call-done, bf16[2048,1408]{1,0:T(8,128)(2,1)} %all-gather.10.cloned.1.call-done), kind=kOutput, calls=%fused_computation.85 | convolution fusion | flops 5905580032 | bytes 15728640 | tf_op jit(solution)/shard_map/dot_general | solution.py:160
  270.7 81.2 %all-gather.12.cloned.1.call-done = bf16[2048,1408]{1,0:T(8,128)(2,1)} async-done(((bf16[256,1408]{1,0:T(8,128)(2,1)}), bf16[2048,1408]{1,0:T(8,128)(2,1)}) %all-gather.12.cloned.1.call-update) | async-done | bytes 5767184 | tf_op jit(solution)/shard_map/all_gather | solution.py:167
  351.9 93.1 %all-gather.14.cloned.1.call-done = bf16[1408,2048]{1,0:T(8,128)(2,1)} async-done(((bf16[1408,256]{1,0:T(8,128)(2,1)}), bf16[1408,2048]{1,0:T(8,128)(2,1)}) %all-gather.14.cloned.1.call-update) | async-done | bytes 5767184 | tf_op jit(solution)/shard_map/all_gather | solution.py:173
  445.0 20.6 %convolution_convert_fusion = bf16[1024,2048]{1,0:T(8,128)(2,1)} fusion(bf16[1408,2048]{1,0:T(8,128)(2,1)} %all-gather.14.cloned.1.call-done, f32[1024,1408]{1,0:T(8,128)} %fusion.49, bf16[1024,2048]{1,0:T(8,128)(2,1)} %all-gather.8.cloned.1.call-done, bf16[2048,1408]{1,0:T(8,128)(2,1)} %all-gather.12.cloned.1.call-done), kind=kOutput, calls=%fused_computation.40 | convolution fusion | flops 11821907968 | bytes 25690112 | tf_op jit(solution)/shard_map/dot_general | solution.py:171
  465.6 43.7 %reduce-scatter.5.cloned.1.call-done = bf16[256,2048]{1,0:T(8,128)(2,1)} async-done(((bf16[1024,2048]{1,0:T(8,128)(2,1)}), bf16[256,2048]{1,0:T(8,128)(2,1)}) %reduce-scatter.5.cloned.1.call-update) | async-done | bytes 1048592 | tf_op jit(solution)/shard_map/reduce_scatter | solution.py:176
  509.2 2.8 fusion.26
  (230 shorter events, 50.5 us)
Async XLA Ops:
  7.4 167.0 %reduce-scatter.3.cloned.1.call-start = ((), (), s32[]{:S(2)}) async-start(), calls=%async_computation.2 | async-start | bytes 5242880 | tf_op jit(solution)/shard_map/reduce_scatter | solution.py:151
  110.2 5.2 %copy-start.3 = (bf16[1024,256]{1,0:T(8,128)(2,1)S(1)}, bf16[1024,256]{1,0:T(8,128)(2,1)}, u32[]{:S(2)}) copy-start(bf16[1024,256]{1,0:T(8,128)(2,1)} %param.21) | copy-start | bytes 1572868
  110.2 5.2 %copy-start.4 = (f32[256]{0:T(256)S(1)}, f32[256]{0:T(256)}, u32[]{:S(2)}) copy-start(f32[256]{0:T(256)} %param.24) | copy-start | bytes 3076
  120.0 54.4 %copy-start = (bf16[256,2048]{1,0:T(8,128)(2,1)S(1)}, bf16[256,2048]{1,0:T(8,128)(2,1)}, u32[]{:S(2)}) copy-start(bf16[256,2048]{1,0:T(8,128)(2,1)} %param.17) | copy-start | bytes 3145732
  120.0 56.1 %copy-start.2 = (f32[2048]{0:T(1024)S(1)}, f32[2048]{0:T(1024)}, u32[]{:S(2)}) copy-start(f32[2048]{0:T(1024)} %param.26) | copy-start | bytes 24580
  120.0 103.7 %all-gather.10.cloned.1.call-start = ((), (), s32[]{:S(2)}) async-start(), calls=%async_computation.4 | async-start | bytes 6488064 | tf_op jit(solution)/shard_map/all_gather | solution.py:162
  120.6 138.4 %all-gather.8.cloned.1.call-start = ((), (), s32[]{:S(2)}) async-start(), calls=%async_computation.3 | async-start | bytes 5242880 | tf_op jit(solution)/shard_map/all_gather | solution.py:159
  178.8 173.1 %all-gather.12.cloned.1.call-start = ((), (), s32[]{:S(2)}) async-start(), calls=%async_computation.5 | async-start | bytes 6488064 | tf_op jit(solution)/shard_map/all_gather | solution.py:167
  179.4 265.6 %all-gather.14.cloned.1.call-start = ((), (), s32[]{:S(2)}) async-start(), calls=%async_computation.6 | async-start | bytes 6488064 | tf_op jit(solution)/shard_map/all_gather | solution.py:173
  180.1 329.1 %reduce-scatter.5.cloned.1.call-start = ((), (), s32[]{:S(2)}) async-start(), calls=%async_computation.7 | async-start | bytes 5242880 | tf_op jit(solution)/shard_map/reduce_scatter | solution.py:176
  465.6 43.7 %copy-start.1 = (bf16[256,2048]{1,0:T(8,128)(2,1)S(1)}, bf16[256,2048]{1,0:T(8,128)(2,1)}, u32[]{:S(2)}) copy-start(bf16[256,2048]{1,0:T(8,128)(2,1)} %reduce-scatter.3.cloned.1.call-done) | copy-start | bytes 3145732
Sparse Core Ops, SparseCore 0:
  120.2 54.1 reduce-scatter.2
  465.7 43.4 reduce-scatter.4
Sparse Core Ops, SparseCore 1:
  122.7 101.0 all-gather.9
  225.2 33.8 all-gather.7
  261.0 90.8 all-gather.11
  353.9 91.0 all-gather.13
where the time goes:
time: 524 us; the launch traced here: 520 us
  waiting for transfers between devices  352 us (67%)
  matrix products  67.3 us (13%)
  blocking collectives  37.8 us (7%)
  other arithmetic  23.2 us (4%)
  local copies, waits for them, and re-layouts  22.2 us (4%)
  between operations  15.2 us (3%)
    all_gather x1, waiting for transfers between devices, on_device(): lax.all_gather(contraction_matrix, 'sp', axis=1, tiled=True)  93.1 us
    all_gather x1, waiting for transfers between devices, on_device(): lax.all_gather(expansion_matrix, 'sp', axis=0, tiled=True)  81.2 us
    reduce_scatter x1, waiting for transfers between devices, on_device(): lax.psum_scatter(jnp.dot(mixed, own_rows, preferred_element_type=jnp.floa...  53.7 us
    reduce_scatter x1, waiting for transfers between devices, on_device(): lax.psum_scatter(partial_sum.astype(jnp.bfloat16), 'tp', scatter_dimensio...  43.7 us
    all_gather x1, waiting for transfers between devices, on_device(): lax.all_gather(switch_matrix, 'sp', axis=0, tiled=True)  43.4 us
    all_gather x2, blocking collectives, carried_in(): lax.all_gather(a.astype(kind), axis)  37.8 us
    all_gather x1, waiting for transfers between devices, on_device(): all_rows = lax.all_gather(normed, 'tp', axis=0, tiled=True)  35.2 us
    dot_general x1, matrix products, on_device(): jnp.dot(hidden, lax.all_gather(contraction_matrix, 'sp', axis=1, tiled=Tr...  20.6 us
  transfers between devices with their start and end apart: 6, of which 6 were waited for; matrix products, arithmetic and copies ran while one was open for 3% of the time, Pallas kernels for 0%

commit v1 on v0

v1 whole, which is shorter than its diff:
```python
import functools

import jax
import jax.numpy as jnp
from jax import lax
from jax.experimental import pallas as pl
from jax.experimental.pallas import tpu as pltpu
from jax.sharding import PartitionSpec as P

HEAD_DIM = 128
BLOCK = 64
STATE_ROWS = HEAD_DIM + 16
EPSILON = 1e-06
MESH = pl.DeviceIdType.MESH
F32, BF16 = jnp.float32, jnp.bfloat16
LAST = (((1,), (1,)), ((), ()))
FIRST = (((0,), (0,)), ((), ()))


def weight_plan(n, me):
    every = (0, 1, 2)
    if n != 8:
        return [[(me, lax.rem(me + d, n), lax.rem(me + n - d, n), every) for d in range(1, n)]]
    ny, nz = 2, n // 2
    z, y = me // ny, lax.rem(me, ny)

    def at(dz, flip):
        return lax.rem(z + dz + nz, nz) * ny + (1 - y if flip else y)

    return [
        [
            (me, at(0, 1), at(0, 1), every),
            (me, at(1, 0), at(-1, 0), every),
            (me, at(-1, 0), at(1, 0), every),
        ],
        [
            (at(1, 0), at(0, 1), at(1, 1), every),
            (at(0, 1), at(1, 0), at(-1, 1), every),
            (at(1, 0), at(-1, 0), at(2, 0), every),
        ],
        [
            (at(2, 0), at(0, 1), at(2, 1), (0,)),
            (at(-1, 1), at(1, 0), at(2, 1), (1,)),
            (at(1, 1), at(-1, 0), at(2, 1), (2,)),
        ],
    ]


def kernel(
    n,
    m,
    skip_ref,
    query_ref,
    forget_ref,
    value_ref,
    emission_ref,
    slack_ref,
    surge_ref,
    gain_ref,
    projection_ref,
    row_gain_ref,
    switch_ref,
    expansion_ref,
    contraction_ref,
    out_ref,
    switch_all,
    expansion_all,
    contraction_all,
    projection,
    stream,
    normed,
    hidden,
    mixed,
    outputs,
    decayed_query,
    state,
    offset,
    state_out,
    state_in,
    part,
    from_buddy,
    cross_out,
    cross_in,
    local_sem,
    weight_send,
    weight_recv,
    skip_send,
    skip_recv,
    mixed_send,
    mixed_recv,
    state_send,
    state_recv,
    buddy_send,
    buddy_recv,
    cross_send,
    cross_recv,
):
    sp, tp = lax.axis_index("sp"), lax.axis_index("tp")
    tokens, width = query_ref.shape
    rows, model = skip_ref.shape
    depth, units = switch_ref.shape
    heads = width // HEAD_DIM
    pairs = m // 2

    barrier = pltpu.get_barrier_semaphore()
    for d in range(1, n):
        pl.semaphore_signal(barrier, inc=1, device_id=(lax.rem(sp + d, n), tp), device_id_type=MESH)
    for d in range(1, m):
        pl.semaphore_signal(barrier, inc=1, device_id=(sp, lax.rem(tp + d, m)), device_id_type=MESH)
    pl.semaphore_wait(barrier, n - 1 + m - 1)

    def remote(src, dst, send, recv, device):
        return pltpu.make_async_remote_copy(
            src_ref=src, dst_ref=dst, send_sem=send, recv_sem=recv, device_id=device, device_id_type=MESH
        )

    own_units = (switch_ref, expansion_ref, contraction_ref)

    def unit(tensor, owner):
        if tensor == 2:
            return contraction_all.at[owner]
        held = (switch_all, expansion_all)[tensor]
        return held.at[pl.ds(pl.multiple_of(owner * depth, depth), depth)]

    plan = weight_plan(n, sp)
    sends = []
    arrivals = []
    index = 0
    for number, step in enumerate(plan):
        sends.append([])
        arrivals.append([])
        for tensor in (0, 1, 2):
            for owner, target, arriving, tensors in step:
                if tensor not in tensors:
                    continue
                src = own_units[tensor] if number == 0 else unit(tensor, owner)
                args = (weight_send.at[index], weight_recv.at[index], (target, tp))
                sends[-1].append(remote(src, unit(tensor, owner), *args))
                arrivals[-1].append(remote(unit(tensor, arriving), unit(tensor, arriving), *args))
                index += 1

    for copy in sends[0]:
        copy.start()

    def rows_of(owner):
        return pl.ds(pl.multiple_of(owner * rows, rows), rows)

    skip_sends, skip_arrivals, mixed_sends, mixed_arrivals = [], [], [], []
    for d in range(1, m):
        source, target = lax.rem(tp + m - d, m), (sp, lax.rem(tp + d, m))
        sems = (skip_send.at[d - 1], skip_recv.at[d - 1], target)
        skip_sends.append(remote(skip_ref, stream.at[rows_of(tp)], *sems))
        skip_arrivals.append(remote(stream.at[rows_of(source)], stream.at[rows_of(source)], *sems))
        sems = (mixed_send.at[d - 1], mixed_recv.at[d - 1], target)
        mixed_sends.append(remote(mixed.at[tp], mixed.at[tp], *sems))
        mixed_arrivals.append(remote(mixed.at[source], mixed.at[source], *sems))
    for copy in skip_sends:
        copy.start()
    local = [
        pltpu.make_async_copy(skip_ref, stream.at[rows_of(tp)], local_sem.at[0]),
        pltpu.make_async_copy(projection_ref, projection, local_sem.at[1]),
    ] + [pltpu.make_async_copy(own_units[t], unit(t, sp), local_sem.at[2 + t]) for t in range(3)]
    for copy in local:
        copy.start()

    state[...] = jnp.zeros_like(state)
    offset[...] = jnp.zeros_like(offset)
    before = lax.broadcasted_iota(jnp.int32, (BLOCK, BLOCK), 0) >= lax.broadcasted_iota(
        jnp.int32, (BLOCK, BLOCK), 1
    )
    lower = before.astype(F32)

    @pl.loop(0, tokens // BLOCK)
    def _(block):
        here = pl.ds(pl.multiple_of(block * BLOCK, BLOCK), BLOCK)
        raw = query_ref[here, :].astype(F32)
        query = raw * jax.nn.sigmoid(raw)
        gate = slack_ref[...] * jax.nn.sigmoid(-forget_ref[here, :].astype(F32))
        log_forget = jnp.log1p(-gate) + surge_ref[here, :]
        total = jnp.dot(lower, log_forget, precision=lax.Precision.HIGHEST, preferred_element_type=F32)
        middle, last = total[BLOCK // 2 : BLOCK // 2 + 1, :], total[BLOCK - 1 :, :]
        left = (query * jnp.exp(total - middle)).astype(BF16)
        right = (gate * jnp.exp(middle - total)).astype(BF16)
        carried = (query * jnp.exp(total)).astype(BF16)
        kept = (gate * jnp.exp(last - total)).astype(BF16)
        decayed_query[here, :] = (query * jnp.exp(total + offset[...])).astype(BF16)
        closing = jnp.exp(last)
        for head in range(heads):
            lanes = slice(head * HEAD_DIM, (head + 1) * HEAD_DIM)
            value = value_ref[here, lanes]
            scores = lax.dot_general(left[:, lanes], right[:, lanes], LAST, preferred_element_type=F32)
            scores = jnp.where(before, scores, 0.0).astype(BF16)
            held = state[head]
            outputs[here, lanes] = jnp.dot(
                scores, value, preferred_element_type=F32
            ) + lax.dot_general(carried[:, lanes], held.astype(BF16), LAST, preferred_element_type=F32)
            state[head] = closing[:, lanes] * held + lax.dot_general(
                value, kept[:, lanes], FIRST, preferred_element_type=F32
            )
        offset[...] += last

    for head in range(heads):
        lanes = slice(head * HEAD_DIM, (head + 1) * HEAD_DIM)
        state_out[head, :HEAD_DIM, :] = state[head].astype(BF16)
        decay = jnp.exp(offset[:, lanes])
        state_out[head, HEAD_DIM:, :] = jnp.broadcast_to(decay, (16, HEAD_DIM)).astype(BF16)
    state_copies = []
    for d in range(1, n):
        copy = remote(
            state_out,
            state_in.at[d - 1],
            state_send.at[d - 1],
            state_recv.at[d - 1],
            (lax.rem(sp + d, n), tp),
        )
        state_copies.append(copy)
        pl.when(sp + d < n)(copy.start)

    if len(plan) > 1:
        for copy in arrivals[0]:
            copy.wait_recv()
        for copy in sends[1]:
            copy.start()

    for d in range(1, n):
        pl.when(sp >= d)(state_copies[d - 1].wait_recv)
    state[...] = jnp.zeros_like(state)

    @pl.loop(0, sp)
    def _(earlier):
        slot = sp - earlier - 1
        for head in range(heads):
            item = state_in[slot, head].astype(F32)
            state[head] = item[HEAD_DIM : HEAD_DIM + 1, :] * state[head] + item[:HEAD_DIM, :]

    tile = min(256, tokens)

    @pl.loop(0, tokens // tile)
    def _(turn):
        here = pl.ds(pl.multiple_of(turn * tile, tile), tile)
        for head in range(heads):
            lanes = slice(head * HEAD_DIM, (head + 1) * HEAD_DIM)
            full = outputs[here, lanes] + lax.dot_general(
                decayed_query[here, lanes], state[head].astype(BF16), LAST, preferred_element_type=F32
            )
            squares = jnp.mean(full * full, axis=-1, keepdims=True)
            raw = emission_ref[here, lanes].astype(F32)
            scaled = full * lax.rsqrt(squares + EPSILON) * gain_ref[:, lanes]
            mixed[tp, here, lanes] = (scaled * (raw * jax.nn.sigmoid(raw))).astype(BF16)

    for copy in mixed_sends:
        copy.start()
    for copy in local:
        copy.wait()
    for copy in skip_arrivals:
        copy.wait_recv()
    for copy in mixed_arrivals:
        copy.wait_recv()

    @pl.loop(0, tokens // tile)
    def _(turn):
        here = pl.ds(pl.multiple_of(turn * tile, tile), tile)
        total = stream[here, :].astype(F32)
        for source in range(m):
            total += jnp.dot(
                mixed[source, here, :],
                projection[source * width : (source + 1) * width, :],
                preferred_element_type=F32,
            )
        rounded = total.astype(BF16)
        stream[here, :] = rounded
        total = rounded.astype(F32)
        squares = jnp.mean(total * total, axis=-1, keepdims=True)
        normed[here, :] = (total * lax.rsqrt(squares + EPSILON) * row_gain_ref[...]).astype(BF16)

    if len(plan) > 1:
        for copy in arrivals[1]:
            copy.wait_recv()
        for copy in sends[2]:
            copy.start()
    for copy in arrivals[-1]:
        copy.wait_recv()

    core, pair = lax.rem(tp, 2), tp // 2
    buddy = (sp, pair * 2 + 1 - core)

    def half(number, which):
        return part.at[number, pl.ds(pl.multiple_of(which * rows, rows), rows)]

    def feed_forward(number, owner):
        inputs = pl.ds(pl.multiple_of(owner * 2 * rows, 2 * rows), 2 * rows)

        def columns(lanes):
            value = normed[inputs, :]
            gate = jnp.dot(value, switch_all[:, lanes], preferred_element_type=F32)
            up = jnp.dot(value, expansion_all[:, lanes], preferred_element_type=F32)
            hidden[:, lanes] = (gate * jax.nn.sigmoid(gate) * up).astype(BF16)

        @pl.loop(0, units // 256)
        def _(turn):
            columns(pl.ds(pl.multiple_of(turn * 256, 256), 256))

        if units % 256:
            columns(slice(units // 256 * 256, units))

        @pl.loop(0, n)
        def _(turn):
            lanes = pl.ds(pl.multiple_of(turn * depth, depth), depth)
            part[number, :, lanes] = jnp.dot(
                hidden[...], contraction_all[turn], preferred_element_type=F32
            ).astype(BF16)

        copy = remote(
            half(number, 1 - core),
            from_buddy.at[number],
            buddy_send.at[number],
            buddy_recv.at[number],
            buddy,
        )
        copy.start()
        return copy

    tail = []
    for d in range(1, pairs):
        owner = lax.rem(pair + d, pairs)
        copy = feed_forward(d, owner)
        copy.wait_recv()
        cross_out[d - 1] = (half(d, core)[...].astype(F32) + from_buddy[d].astype(F32)).astype(BF16)
        cross = remote(
            cross_out.at[d - 1],
            cross_in.at[d - 1],
            cross_send.at[d - 1],
            cross_recv.at[d - 1],
            (sp, owner * 2 + core),
        )
        cross.start()
        tail += [copy, cross]
    copy = feed_forward(0, pair)
    copy.wait_recv()
    total = half(0, core)[...].astype(F32) + from_buddy[0].astype(F32) + stream[rows_of(tp), :].astype(F32)
    for d in range(1, pairs):
        tail[2 * d - 1].wait_recv()
        total += cross_in[d - 1].astype(F32)
    out_ref[...] = total.astype(BF16)

    for copy in tail + [copy] + skip_sends + mixed_sends + [c for step in sends for c in step]:
        copy.wait_send()
    for d in range(1, n):
        pl.when(sp + d < n)(state_copies[d - 1].wait_send)


def on_device(n, m, *arrays):
    (skip, query, forget, value, emission, slack, surge, gain, projection, row_gain, switch, expansion, contraction) = arrays
    tokens, width = query.shape
    rows, model = skip.shape
    depth, units = switch.shape
    heads, pairs = width // HEAD_DIM, m // 2
    count = 21 if n == 8 else 3 * (n - 1)
    vmem, anywhere = pl.BlockSpec(memory_space=pltpu.VMEM), pl.BlockSpec(memory_space=pl.ANY)
    dma = pltpu.SemaphoreType.DMA
    return pl.pallas_call(
        functools.partial(kernel, n, m),
        out_shape=jax.ShapeDtypeStruct((rows, model), BF16),
        in_specs=[anywhere] + [vmem] * 7 + [anywhere, vmem] + [anywhere] * 3,
        out_specs=vmem,
        scratch_shapes=[
            pltpu.VMEM((model, units), BF16),
            pltpu.VMEM((model, units), BF16),
            pltpu.VMEM((n, units, depth), BF16),
            pltpu.VMEM(projection.shape, BF16),
            pltpu.VMEM((tokens, model), BF16),
            pltpu.VMEM((tokens, model), BF16),
            pltpu.VMEM((2 * rows, units), BF16),
            pltpu.VMEM((m, tokens, width), BF16),
            pltpu.VMEM((tokens, width), F32),
            pltpu.VMEM((tokens, width), BF16),
            pltpu.VMEM((heads, HEAD_DIM, HEAD_DIM), F32),
            pltpu.VMEM((1, width), F32),
            pltpu.VMEM((heads, STATE_ROWS, HEAD_DIM), BF16),
            pltpu.VMEM((n - 1, heads, STATE_ROWS, HEAD_DIM), BF16),
            pltpu.VMEM((pairs, 2 * rows, model), BF16),
            pltpu.VMEM((pairs, rows, model), BF16),
            pltpu.VMEM((pairs - 1, rows, model), BF16),
            pltpu.VMEM((pairs - 1, rows, model), BF16),
            dma((5,)),
            dma((count,)),
            dma((count,)),
            dma((m - 1,)),
            dma((m - 1,)),
            dma((m - 1,)),
            dma((m - 1,)),
            dma((n - 1,)),
            dma((n - 1,)),
            dma((pairs,)),
            dma((pairs,)),
            dma((pairs - 1,)),
            dma((pairs - 1,)),
        ],
        compiler_params=pltpu.CompilerParams(
            collective_id=0, has_side_effects=True, vmem_limit_bytes=63_000_000
        ),
    )(
        skip,
        query,
        forget,
        value,
        emission,
        slack.reshape(1, width),
        surge,
        gain.reshape(1, width),
        projection,
        row_gain.reshape(1, model),
        switch,
        expansion,
        contraction,
    )


def solution(mesh):
    in_specs = (
        P(("sp", "tp"), None),
        P("sp", "tp"),
        P("sp", "tp"),
        P("sp", "tp"),
        P("sp", "tp"),
        P("tp"),
        P("sp", "tp"),
        P("tp"),
        P(),
        P(),
        P("sp", "tp"),
        P("sp", "tp"),
        P("tp", "sp"),
    )
    return jax.shard_map(
        functools.partial(on_device, mesh.shape["sp"], mesh.shape["tp"]),
        mesh=mesh,
        in_specs=in_specs,
        out_specs=P(("sp", "tp"), None),
        check_vma=False,
    )
```

time: 524 us -> 280 us (0.53)
  waiting for transfers between devices: 352 us -> 0 us
  Pallas kernels: 0 us -> 274 us
  matrix products: 67.3 us -> 0 us
  blocking collectives: 37.8 us -> 0 us
  other arithmetic: 23.2 us -> 0 us
  local copies, waits for them, and re-layouts: 22.2 us -> 2.3 us
  between operations: 15.2 us -> 0.01 us
    pallas_call x0 -> x1, Pallas kernels: none -> 274 us  [on_device(): pl.pallas_call(functools.partial(kernel, n, m), out_shape=jax.ShapeDtypeS...]
    all_gather x4 -> x0, waiting for transfers between devices: 253 us -> none  [the longest x1 93.1 us: on_device(): lax.all_gather(contraction_matrix, 'sp', axis=1, tiled=True)]
    reduce_scatter x2 -> x0, waiting for transfers between devices: 97.4 us -> none  [the longest x1 53.7 us: on_device(): lax.psum_scatter(jnp.dot(mixed, own_rows, preferred_element_type=jnp.floa...]
    dot_general x68 -> x0, matrix products: 67.3 us -> none  [the longest x1 20.6 us: on_device(): jnp.dot(hidden, lax.all_gather(contraction_matrix, 'sp', axis=1, tiled=Tr...]
    all_gather x2 -> x0, blocking collectives: 37.8 us -> none  [carried_in(): lax.all_gather(a.astype(kind), axis)]
    dynamic_slice x48 -> x0, local copies, waits for them, and re-layouts: 14.5 us -> none  [on_device(): lax.scan(block_step, start_carry, block_list)]
    dynamic_update_slice x16 -> x0, other arithmetic: 9.98 us -> none  [on_device(): lax.scan(block_step, start_carry, block_list)]
    convert_element_type x9 -> x0, other arithmetic: 5.42 us -> none  [the longest x1 2.78 us: on_device(): return (stream.astype(jnp.float32) + summed).astype(jnp.bfloat16)]
  transfers between devices with their start and end apart: 6 -> 0, of which waited for: 6 -> 0; matrix products, arithmetic and copies ran while one was open for 3% -> 0% of each run, Pallas kernels for 0% -> 0%
where the time goes in v1:
time: 280 us; the launch traced here: 277 us
  Pallas kernels  274 us (98%)
    pallas_call x1, Pallas kernels, on_device(): pl.pallas_call(functools.partial(kernel, n, m), out_shape=jax.ShapeDtypeS...  274 us

profile of v1, /device:TPU:27, one launch (start us, length us, event | category | flops | bytes accessed | tf_op | source)
XLA Modules:
  0.0 276.7 jit_solution(13073898318119475020)
XLA Ops:
  0.0 274.3 %shard_map.127 = bf16[256,2048]{1,0:T(8,128)(2,1)} custom-call(bf16[256,2048]{1,0:T(8,128)(2,1)} %skip_ref.1, bf16[1024,256]{1,0:T(8,128)(2,1)} %query_ref.1, bf16[1024,256]{1,0:T(8,128)(2,1)} %forget_ref.1, bf16[1024,256]{1,0:T(8,128)(2,1)} %value_ref.1, bf16[1024,256]{1,0:T(8,128)(2,1)} %emission_ref.1, f32[1,256]{1,0:T(1,128)} %bitcast.4, ...), custom_call_target="tpu_custom_call" | custom-call | tf_op jit(solution)/shard_map/pallas_call | solution.py:361
  274.4 2.3 copy.15

commit v2 on v1

--- a/solution.py
+++ b/solution.py
@@ -18,32 +18,50 @@
 
 
 def weight_plan(n, me):
-    every = (0, 1, 2)
+    out = []
     if n != 8:
-        return [[(me, lax.rem(me + d, n), lax.rem(me + n - d, n), every) for d in range(1, n)]]
+        for tensor in range(3):
+            for d in range(1, n):
+                to, source = lax.rem(me + d, n), lax.rem(me + n - d, n)
+                out.append((0, tensor, ("D", d, tensor), True, me, to, True, source, None))
+        return out
     ny, nz = 2, n // 2
     z, y = me // ny, lax.rem(me, ny)
 
-    def at(dz, flip):
-        return lax.rem(z + dz + nz, nz) * ny + (1 - y if flip else y)
-
-    return [
-        [
-            (me, at(0, 1), at(0, 1), every),
-            (me, at(1, 0), at(-1, 0), every),
-            (me, at(-1, 0), at(1, 0), every),
-        ],
-        [
-            (at(1, 0), at(0, 1), at(1, 1), every),
-            (at(0, 1), at(1, 0), at(-1, 1), every),
-            (at(1, 0), at(-1, 0), at(2, 0), every),
-        ],
-        [
-            (at(2, 0), at(0, 1), at(2, 1), (0,)),
-            (at(-1, 1), at(1, 0), at(2, 1), (1,)),
-            (at(1, 1), at(-1, 0), at(2, 1), (2,)),
-        ],
-    ]
+    def at(place, flip):
+        return jnp.clip(place, 0, nz - 1) * ny + (1 - y if flip else y)
+
+    def crossed(place, tensor, way):
+        first, last = (1, nz - 1) if way > 0 else (nz - 2, 0)
+        return (place == first) | (place == last) if tensor == 0 else place == first
+
+    def inside(place):
+        return (place >= 0) & (place < nz)
+
+    for tensor in range(3):
+        late = 1 if tensor == 2 else 0
+        out.append((0, tensor, ("Y", 0, tensor), True, me, at(z, 1), True, at(z, 1), None))
+        for way in (1, -1):
+            for k in range(1, nz):
+                to, unit = z + way, z + way - way * k
+                name, above = (way, k, tensor), (way, k - 1, tensor)
+                stage = 0 if k == 1 else k - 1 + late
+                out.append(
+                    (stage, tensor, name, inside(to) & inside(unit), at(unit, 0), at(to, 0),
+                     inside(z - way * k), at(z - way * k, 0), None if k == 1 else above)
+                )
+                held = inside(z - way * k)
+                if k == 1:
+                    held = held & jnp.logical_not(crossed(z, tensor, way))
+                out.append(
+                    (k + late, tensor, ("Y", way * k, tensor), held, at(z - way * k, 0), at(z, 1),
+                     held, at(z - way * k, 1), name)
+                )
+            out.append(
+                (2, tensor, ("X", way, tensor), inside(z + way) & crossed(z + way, tensor, way), at(z, 1),
+                 at(z + way, 0), crossed(z, tensor, way), at(z - way, 1), ("Y", 0, tensor))
+            )
+    return out
 
 
 def kernel(
@@ -122,25 +140,36 @@
         held = (switch_all, expansion_all)[tensor]
         return held.at[pl.ds(pl.multiple_of(owner * depth, depth), depth)]
 
-    plan = weight_plan(n, sp)
-    sends = []
-    arrivals = []
-    index = 0
-    for number, step in enumerate(plan):
-        sends.append([])
-        arrivals.append([])
-        for tensor in (0, 1, 2):
-            for owner, target, arriving, tensors in step:
-                if tensor not in tensors:
-                    continue
-                src = own_units[tensor] if number == 0 else unit(tensor, owner)
-                args = (weight_send.at[index], weight_recv.at[index], (target, tp))
-                sends[-1].append(remote(src, unit(tensor, owner), *args))
-                arrivals[-1].append(remote(unit(tensor, arriving), unit(tensor, arriving), *args))
-                index += 1
-
-    for copy in sends[0]:
-        copy.start()
+    messages = {}
+    for index, (stage, tensor, name, sent, owner, target, arrives, arriving, after) in enumerate(
+        weight_plan(n, sp)
+    ):
+        src = own_units[tensor] if stage == 0 else unit(tensor, owner)
+        args = (weight_send.at[index], weight_recv.at[index], (target, tp))
+        send = remote(src, unit(tensor, owner), *args)
+        arrival = remote(unit(tensor, arriving), unit(tensor, arriving), *args)
+        messages[name] = (stage, sent, send, arrives, arrival, after)
+    arrived = set()
+
+    def where(condition, action):
+        if condition is True:
+            action()
+        else:
+            pl.when(condition)(action)
+
+    def await_unit(name):
+        if name not in arrived:
+            arrived.add(name)
+            where(messages[name][3], messages[name][4].wait_recv)
+
+    def run_stage(wanted):
+        for name, (stage, sent, send, _, _, after) in messages.items():
+            if stage == wanted:
+                if after is not None:
+                    await_unit(after)
+                where(sent, send.start)
+
+    run_stage(0)
 
     def rows_of(owner):
         return pl.ds(pl.multiple_of(owner * rows, rows), rows)
@@ -216,11 +245,7 @@
         state_copies.append(copy)
         pl.when(sp + d < n)(copy.start)
 
-    if len(plan) > 1:
-        for copy in arrivals[0]:
-            copy.wait_recv()
-        for copy in sends[1]:
-            copy.start()
+    run_stage(1)
 
     for d in range(1, n):
         pl.when(sp >= d)(state_copies[d - 1].wait_recv)
@@ -250,6 +275,7 @@
 
     for copy in mixed_sends:
         copy.start()
+    run_stage(2)
     for copy in local:
         copy.wait()
     for copy in skip_arrivals:
@@ -273,13 +299,10 @@
         squares = jnp.mean(total * total, axis=-1, keepdims=True)
         normed[here, :] = (total * lax.rsqrt(squares + EPSILON) * row_gain_ref[...]).astype(BF16)
 
-    if len(plan) > 1:
-        for copy in arrivals[1]:
-            copy.wait_recv()
-        for copy in sends[2]:
-            copy.start()
-    for copy in arrivals[-1]:
-        copy.wait_recv()
+    run_stage(3)
+    for name in messages:
+        if name[2] < 2:
+            await_unit(name)
 
     core, pair = lax.rem(tp, 2), tp // 2
     buddy = (sp, pair * 2 + 1 - core)
@@ -287,14 +310,14 @@
     def half(number, which):
         return part.at[number, pl.ds(pl.multiple_of(which * rows, rows), rows)]
 
-    def feed_forward(number, owner):
+    def gate_and_up(number, owner):
         inputs = pl.ds(pl.multiple_of(owner * 2 * rows, 2 * rows), 2 * rows)
 
         def columns(lanes):
             value = normed[inputs, :]
             gate = jnp.dot(value, switch_all[:, lanes], preferred_element_type=F32)
             up = jnp.dot(value, expansion_all[:, lanes], preferred_element_type=F32)
-            hidden[:, lanes] = (gate * jax.nn.sigmoid(gate) * up).astype(BF16)
+            hidden[number, :, lanes] = (gate * jax.nn.sigmoid(gate) * up).astype(BF16)
 
         @pl.loop(0, units // 256)
         def _(turn):
@@ -303,11 +326,12 @@
         if units % 256:
             columns(slice(units // 256 * 256, units))
 
+    def down(number):
         @pl.loop(0, n)
         def _(turn):
             lanes = pl.ds(pl.multiple_of(turn * depth, depth), depth)
             part[number, :, lanes] = jnp.dot(
-                hidden[...], contraction_all[turn], preferred_element_type=F32
+                hidden[number], contraction_all[turn], preferred_element_type=F32
             ).astype(BF16)
 
         copy = remote(
@@ -320,10 +344,15 @@
         copy.start()
         return copy
 
+    for d in [*range(1, pairs), 0]:
+        gate_and_up(d, lax.rem(pair + d, pairs))
+    run_stage(4)
+    for name in messages:
+        await_unit(name)
     tail = []
     for d in range(1, pairs):
         owner = lax.rem(pair + d, pairs)
-        copy = feed_forward(d, owner)
+        copy = down(d)
         copy.wait_recv()
         cross_out[d - 1] = (half(d, core)[...].astype(F32) + from_buddy[d].astype(F32)).astype(BF16)
         cross = remote(
@@ -335,7 +364,7 @@
         )
         cross.start()
         tail += [copy, cross]
-    copy = feed_forward(0, pair)
+    copy = down(0)
     copy.wait_recv()
     total = half(0, core)[...].astype(F32) + from_buddy[0].astype(F32) + stream[rows_of(tp), :].astype(F32)
     for d in range(1, pairs):
@@ -343,8 +372,10 @@
         total += cross_in[d - 1].astype(F32)
     out_ref[...] = total.astype(BF16)
 
-    for copy in tail + [copy] + skip_sends + mixed_sends + [c for step in sends for c in step]:
+    for copy in tail + [copy] + skip_sends + mixed_sends:
         copy.wait_send()
+    for _, sent, send, _, _, _ in messages.values():
+        where(sent, send.wait_send)
     for d in range(1, n):
         pl.when(sp + d < n)(state_copies[d - 1].wait_send)
 
@@ -355,7 +386,7 @@
     rows, model = skip.shape
     depth, units = switch.shape
     heads, pairs = width // HEAD_DIM, m // 2
-    count = 21 if n == 8 else 3 * (n - 1)
+    count = 3 * (3 * n // 2 + 3) if n == 8 else 3 * (n - 1)
     vmem, anywhere = pl.BlockSpec(memory_space=pltpu.VMEM), pl.BlockSpec(memory_space=pl.ANY)
     dma = pltpu.SemaphoreType.DMA
     return pl.pallas_call(
@@ -370,7 +401,7 @@
             pltpu.VMEM(projection.shape, BF16),
             pltpu.VMEM((tokens, model), BF16),
             pltpu.VMEM((tokens, model), BF16),
-            pltpu.VMEM((2 * rows, units), BF16),
+            pltpu.VMEM((pairs, 2 * rows, units), BF16),
             pltpu.VMEM((m, tokens, width), BF16),
             pltpu.VMEM((tokens, width), F32),
             pltpu.VMEM((tokens, width), BF16),

time: 280 us -> 221 us (0.79); the launches traced: 277 us -> 221 us
  Pallas kernels: 274 us -> 219 us
    pallas_call x1, Pallas kernels: 274 us -> 219 us  [on_device(): pl.pallas_call(functools.partial(kernel, n, m), out_shape=jax.ShapeDtypeS...]
where the time goes in v2:
time: 221 us
  Pallas kernels  219 us (99%)
  local copies, waits for them, and re-layouts  2.3 us (1%)
    pallas_call x1, Pallas kernels, on_device(): pl.pallas_call(functools.partial(kernel, n, m), out_shape=jax.ShapeDtypeS...  219 us

profile of v2, /device:TPU:27, one launch (start us, length us, event | category | flops | bytes accessed | tf_op | source)
XLA Modules:
  0.0 220.8 jit_solution(17008401886491258566)
XLA Ops:
  0.0 218.5 %shard_map.127 = bf16[256,2048]{1,0:T(8,128)(2,1)} custom-call(bf16[256,2048]{1,0:T(8,128)(2,1)} %skip_ref.1, bf16[1024,256]{1,0:T(8,128)(2,1)} %query_ref.1, bf16[1024,256]{1,0:T(8,128)(2,1)} %forget_ref.1, bf16[1024,256]{1,0:T(8,128)(2,1)} %value_ref.1, bf16[1024,256]{1,0:T(8,128)(2,1)} %emission_ref.1, f32[1,256]{1,0:T(1,128)} %bitcast.4, ...), custom_call_target="tpu_custom_call" | custom-call | tf_op jit(solution)/shard_map/pallas_call | solution.py:392
  218.5 2.3 %copy.15 = bf16[256,2048]{1,0:T(8,128)(2,1)} copy(bf16[256,2048]{1,0:T(8,128)(2,1)} %shard_map.127) | data formatting | bytes 2097152
